TPU v7x, 32 devices: a whole 2x2x4 slice. The times are simulated.
32 devices in a mesh: grp: 2 (over x), tp: 4 (over z), dp: 4 (over y, core).
Axes of the slice: x: 2, y: 2, z: 4, core: 2. Of those that a mesh axis runs over, the one named last changes fastest.
Arguments:
- stream: bfloat16 [32, 4096], P('grp', 'dp'), parts along dimension 0, may hold values from -11 to 11
- states: float32 [2, 32, 32, 64, 64], P(None, ('grp', 'dp'), 'tp'), parts along dimension 1, may hold values from -6 to 6
- norm_gain: bfloat16 [2, 4096], P(None, 'dp'), may hold values from 0.099609375 to 1.8984375
- recept_weight: bfloat16 [2, 4096, 2048], P(None, 'dp', 'tp'), may hold values from -0.09375 to 0.09375
- key_weight: bfloat16 [2, 4096, 2048], P(None, 'dp', 'tp'), may hold values from -0.09375 to 0.09375
- value_weight: bfloat16 [2, 4096, 2048], P(None, 'dp', 'tp'), may hold values from -0.09375 to 0.09375
- decay_weight: bfloat16 [2, 4096, 2048], P(None, 'dp', 'tp'), may hold values from -0.09375 to 0.09375
- rate_weight: bfloat16 [2, 4096, 2048], P(None, 'dp', 'tp'), may hold values from -0.09375 to 0.09375
- gate_weight: bfloat16 [2, 4096, 2048], P(None, 'dp', 'tp'), may hold values from -0.09375 to 0.09375
- out_weight: bfloat16 [2, 2048, 4096], P(None, 'tp', 'dp'), may hold values from -0.125 to 0.125
- decay_bias: float32 [2, 2048], P(None, 'tp'), may hold values from -2 to 2
- head_gain: bfloat16 [2, 2048], P(None, 'tp'), may hold values from 0.099609375 to 1.8984375
Outputs:
- new_stream: bfloat16 [32, 4096], P('grp', 'dp'), parts along dimension 0
- new_states: float32 [2, 32, 32, 64, 64], P(None, ('grp', 'dp'), 'tp'), parts along dimension 1
There are 2 independent parts, one for each index of `grp`. A program takes and returns all parts, laid end to end along the dimension named above; an argument that names none is the same for every part. Nothing has to cross between parts.
All inputs are finite; a program needn't handle non-finite values.
Results may differ from a plain program's by a relative error of at most 0.0068.
Values may be sent and summed in bfloat16 or wider, within the bound.
A program may use at most 64 MiB of HBM per device.

v0:
```python
import jax
import jax.numpy as jnp
from jax import lax
from jax.sharding import PartitionSpec as P

D = 4096
HEAD = 64


def run_block(stream, state_blk, gain, weights, out_weight, bias, hgain):
    current = stream.astype(jnp.float32)
    squares = jnp.sum(current * current, axis=1)
    normed = (current * gain.astype(jnp.float32)).astype(jnp.bfloat16)
    width = weights[0].shape[1]
    local_rows = state_blk.shape[0]
    all_totals = lax.psum(squares, "dp")
    offset = lax.axis_index("dp") * local_rows
    totals = lax.dynamic_slice_in_dim(all_totals, offset, local_rows, 0)
    summed = lax.psum_scatter(
        jnp.concatenate(
            [jnp.dot(normed, weight, preferred_element_type=jnp.float32) for weight in weights],
            axis=1,
        ),
        "dp",
        scatter_dimension=0,
        tiled=True,
    )
    inv_rms = lax.rsqrt(totals / D + 1e-06)[:, None]
    projected = (summed * inv_rms).reshape(local_rows, 6, -1, HEAD)
    recept = projected[:, 0]
    key_vec = projected[:, 1]
    value_vec = projected[:, 2]
    decay_pre = projected[:, 3]
    rate_pre = projected[:, 4]
    gate_pre = projected[:, 5]
    unit_key = key_vec * lax.rsqrt(jnp.sum(key_vec * key_vec, axis=2, keepdims=True) + 1e-06)
    rate_vec = jax.nn.sigmoid(rate_pre)
    decay = jnp.exp(-0.606531 * jax.nn.sigmoid(bias.reshape(1, -1, HEAD) + decay_pre))
    removed = jnp.einsum("bhij,bhj->bhi", state_blk, unit_key, precision=lax.Precision.HIGHEST)
    new_state = (
        state_blk * decay[:, :, None, :]
        - removed[..., None] * (unit_key * rate_vec)[:, :, None, :]
        + value_vec[..., None] * key_vec[:, :, None, :]
    )
    read = jnp.einsum("bhij,bhj->bhi", new_state, recept, precision=lax.Precision.HIGHEST)
    center = read - jnp.mean(read, axis=2, keepdims=True)
    normal_read = center * lax.rsqrt(jnp.mean(center * center, axis=2, keepdims=True) + 1e-05)
    gated = normal_read * hgain.astype(jnp.float32).reshape(1, -1, HEAD) * jax.nn.sigmoid(gate_pre)
    mixed = gated.reshape(local_rows, width).astype(jnp.bfloat16)
    branch_part = jnp.dot(
        lax.all_gather(mixed, "dp", axis=0, tiled=True),
        out_weight,
        preferred_element_type=jnp.float32,
    )
    branch = lax.psum(branch_part, "tp")
    return ((current + branch).astype(jnp.bfloat16), new_state)


def per_device(
    stream,
    states,
    norm_gain,
    recept_weight,
    key_weight,
    value_weight,
    decay_weight,
    rate_weight,
    gate_weight,
    out_weight,
    decay_bias,
    head_gain,
):
    current = stream
    fresh_list = []
    for layer in range(2):
        weights = (
            recept_weight[layer],
            key_weight[layer],
            value_weight[layer],
            decay_weight[layer],
            rate_weight[layer],
            gate_weight[layer],
        )
        current, fresh = run_block(
            current,
            states[layer],
            norm_gain[layer],
            weights,
            out_weight[layer],
            decay_bias[layer],
            head_gain[layer],
        )
        fresh_list.append(fresh)
    return (current, jnp.stack(fresh_list))


def solution(mesh):
    in_specs = (
        P("grp", "dp"),
        P(None, ("grp", "dp"), "tp", None, None),
        P(None, "dp"),
        P(None, "dp", "tp"),
        P(None, "dp", "tp"),
        P(None, "dp", "tp"),
        P(None, "dp", "tp"),
        P(None, "dp", "tp"),
        P(None, "dp", "tp"),
        P(None, "tp", "dp"),
        P(None, "tp"),
        P(None, "tp"),
    )
    out_specs = (P("grp", "dp"), P(None, ("grp", "dp"), "tp", None, None))
    return jax.shard_map(
        per_device, mesh=mesh, in_specs=in_specs, out_specs=out_specs, check_vma=False
    )
```

profile of v0, /device:TPU:0, one launch (start us, length us, event | category | flops | bytes accessed | tf_op | source)
XLA Modules:
  0.0 201.3 jit_solution(15151777179491624203)
XLA Ops:
  7.2 0.0 all-reduce.11.cloned.1.call-start
  7.2 0.9 slice_convert_fusion
  8.1 1.6 convolution_dynamic-update-slice_fusion.11
  9.7 1.5 convolution_dynamic-update-slice_fusion.10
  11.3 0.2 convolution_dynamic-update-slice_fusion.9
  11.5 1.6 convolution_dynamic-update-slice_fusion.8
  13.1 0.3 convolution_dynamic-update-slice_fusion.7
  13.4 1.5 convolution_dynamic-update-slice_fusion.6
  14.9 0.7 copy-done.6
  15.6 0.0 all-reduce.11.cloned.1.call-update
  15.6 0.0 all-reduce.7.cloned.1.call-start
  15.6 0.1 fusion.61
  15.8 8.4 %psum.28 = f32[16]{0:T(128)S(1)} all-reduce(f32[16]{0:T(128)S(1)} %fusion.61), channel_id=1, replica_groups=mesh['grp'=2,'tp'=4,'dp'=4] {'dp'}, use_global_device_ids=true, to_apply=%region_2.0 | all-reduce | flops 16 | bytes 128 | tf_op jit(solution)/shard_map/psum | solution.py:16
  24.2 0.1 reshape.165
  24.3 0.1 add.138
  24.4 0.6 dynamic-slice
  25.6 0.1 add_rsqrt_fusion.5
  25.7 24.8 %all-reduce.11.cloned.1.call-done = f32[16,3072]{1,0:T(8,128)} async-done(((f32[16,3072]{1,0:T(8,128)}), f32[16,3072]{1,0:T(8,128)}) %all-reduce.11.cloned.1.call-update) | async-done | bytes 196624
  50.5 1.0 dynamic-slice_multiply_fusion.1
  51.4 0.1 reshape.162
  51.5 0.1 fusion.99
  51.6 0.1 fusion.92
  51.7 1.7 fusion.22
  53.5 2.1 %fusion.26 = f32[4,8,1,64]{3,2,1,0:T(1,128)S(1)} fusion(f32[4,8,64,1]{2,3,1,0:T(1,128)S(1)} %bitcast.192, f32[2,4,8,64,64]{4,3,2,1,0:T(8,128)S(1)} %copy-done, f32[4,8,64]{2,1,0:T(8,128)S(1)} %get-tuple-element.23, f32[4,8,64]{2,1,0:T(8,128)S(1)} %get-tuple-element.21, f32[4,8,64]{2,1,0:T(8,128)S(1)} %get-tuple-element.10, f32[4,8,64]{2,1,0:T(8,128)S(1)} %bitcast.185, ...), kind=kOutput, calls=%fused_computation.40 | convolution fusion | flops 2228224 | bytes 1155072 | tf_op jit(solution)/shard_map/bhij,bhj->bhi/dot_general | solution.py:45
  55.5 0.1 reduce_sum.74
  55.6 0.2 multiply_reduce_fusion.2
  55.8 0.1 fusion.100
  55.9 0.1 reshape.168
  56.0 5.2 %all-gather = bf16[4,4,512]{2,1,0:T(4,128)(2,1)S(1)} all-gather(bf16[1,4,512]{2,1,0:T(4,128)(2,1)S(1)} %reshape.168), channel_id=1, replica_groups=mesh['grp'=2,'tp'=4,'dp'=4] {'dp'}, dimensions={0}, use_global_device_ids=true | all-gather | bytes 20480 | tf_op jit(solution)/shard_map/all_gather | solution.py:51
  61.2 2.1 %fusion.14 = f32[16,1024]{1,0:T(8,128)} fusion(bf16[16,512]{1,0:T(8,128)(2,1)S(1)} %reshape.169, bf16[2,512,1024]{2,1,0:T(8,128)(2,1)} %param.21), kind=kOutput, calls=%fused_computation.27 | convolution fusion | flops 16777216 | bytes 1130496 | tf_op jit(solution)/shard_map/dot_general | solution.py:50
  63.3 0.0 all-reduce.13.cloned.1.call-start
  63.4 0.1 reshape.167
  63.5 0.1 add.150
  63.5 34.3 %all-reduce.7.cloned.1.call-done = f32[16,1024]{1,0:T(8,128)} async-done(((f32[16,1024]{1,0:T(8,128)}), f32[16,1024]{1,0:T(8,128)}) %all-reduce.7.cloned.1.call-update) | async-done | bytes 65552 | tf_op jit(solution)/shard_map/psum | solution.py:55
  97.8 1.0 fusion.64
  98.8 5.7 %psum.30 = f32[16]{0:T(128)S(1)} all-reduce(f32[16]{0:T(128)S(1)} %get-tuple-element.8), channel_id=1, replica_groups=mesh['grp'=2,'tp'=4,'dp'=4] {'dp'}, use_global_device_ids=true, to_apply=%region_9.0 | all-reduce | flops 16 | bytes 128 | tf_op jit(solution)/shard_map/psum | solution.py:16
  104.4 1.6 convolution_dynamic-update-slice_fusion.5
  106.1 1.5 convolution_dynamic-update-slice_fusion.4
  107.5 0.3 convolution_dynamic-update-slice_fusion.3
  107.8 1.5 convolution_dynamic-update-slice_fusion.2
  109.3 0.3 convolution_dynamic-update-slice_fusion.1
  109.5 1.5 convolution_dynamic-update-slice_fusion
  111.0 0.7 copy-done.7
  111.7 0.0 all-reduce.13.cloned.1.call-update
  111.7 0.0 all-reduce.9.cloned.1.call-start
  111.8 0.1 add_rsqrt_fusion.4
  111.8 32.0 %all-reduce.13.cloned.1.call-done = f32[16,3072]{1,0:T(8,128)} async-done(((f32[16,3072]{1,0:T(8,128)}), f32[16,3072]{1,0:T(8,128)}) %all-reduce.13.cloned.1.call-update) | async-done | bytes 196624
  143.8 1.0 dynamic-slice_multiply_fusion
  144.8 0.1 reshape.163
  144.9 0.1 fusion.82
  145.0 0.1 fusion.75
  145.1 1.7 fusion.8
  146.8 2.2 %multiply_add_fusion.1 = (f32[1,4,8,64,64]{4,3,2,1,0:T(8,128)S(1)}, f32[1,4,8,64,64]{4,3,2,1,0:T(8,128)}) fusion(f32[2,4,8,64,64]{4,3,2,1,0:T(8,128)S(1)} %copy-done, f32[4,8,64]{2,1,0:T(8,128)S(1)} %get-tuple-element.23, f32[4,8,64]{2,1,0:T(8,128)S(1)} %get-tuple-element.21, f32[4,8,64]{2,1,0:T(8,128)S(1)} %get-tuple-element.10, ...), kind=kLoop, calls=%fused_computation.42 | loop fusion | flops 1310720 | bytes 2179072 | tf_op jit(solution)/shard_map/add | solution.py:41
  149.0 2.1 %fusion.12 = f32[4,8,1,64]{3,2,1,0:T(1,128)S(1)} fusion(f32[4,8,64,1]{2,3,1,0:T(1,128)S(1)} %bitcast.191, f32[2,4,8,64,64]{4,3,2,1,0:T(8,128)S(1)} %copy-done, f32[4,8,64]{2,1,0:T(8,128)S(1)} %get-tuple-element.18, f32[4,8,64]{2,1,0:T(8,128)S(1)} %get-tuple-element.16, f32[4,8,64]{2,1,0:T(8,128)S(1)} %get-tuple-element.6, f32[4,8,64]{2,1,0:T(8,128)S(1)} %bitcast.188, ...), kind=kOutput, calls=%fused_computation.26 | convolution fusion | flops 2228224 | bytes 1155072 | tf_op jit(solution)/shard_map/bhij,bhj->bhi/dot_general | solution.py:45
  151.1 0.1 reduce_sum.78
  151.2 0.2 multiply_reduce_fusion
  151.4 0.1 fusion.101
  151.4 0.1 reshape.170
  151.5 5.2 %all-gather.1 = bf16[4,4,512]{2,1,0:T(4,128)(2,1)S(1)} all-gather(bf16[1,4,512]{2,1,0:T(4,128)(2,1)S(1)} %reshape.170), channel_id=1, replica_groups=mesh['grp'=2,'tp'=4,'dp'=4] {'dp'}, dimensions={0}, use_global_device_ids=true | all-gather | bytes 20480 | tf_op jit(solution)/shard_map/all_gather | solution.py:51
  156.8 2.1 %fusion = f32[16,1024]{1,0:T(8,128)} fusion(bf16[16,512]{1,0:T(8,128)(2,1)S(1)} %reshape.171, bf16[2,512,1024]{2,1,0:T(8,128)(2,1)} %param.21), kind=kOutput, calls=%fused_computation.13 | convolution fusion | flops 16777216 | bytes 1130496 | tf_op jit(solution)/shard_map/dot_general | solution.py:50
  158.8 0.0 all-reduce.9.cloned.1.call-update
  158.9 2.8 %pad_maximum_fusion = f32[2,4,8,64,64]{4,3,2,1,0:T(8,128)} fusion(f32[1,4,8,64,64]{4,3,2,1,0:T(8,128)} %get-tuple-element.13, f32[1,4,8,64,64]{4,3,2,1,0:T(8,128)S(1)} %get-tuple-element.12), kind=kLoop, calls=%fused_computation | loop fusion | flops 262144 | bytes 2097152 | tf_op jit(solution)/shard_map/stack | solution.py:94
  161.6 31.7 %all-reduce.9.cloned.1.call-done = f32[16,1024]{1,0:T(8,128)} async-done(((f32[16,1024]{1,0:T(8,128)}), f32[16,1024]{1,0:T(8,128)}) %all-reduce.9.cloned.1.call-update) | async-done | bytes 65552 | tf_op jit(solution)/shard_map/psum | solution.py:55
  193.3 1.5 fusion.65
  (32 shorter events, 0.2 us)
Async XLA Ops:
  7.2 4.1 %copy-start.1 = (bf16[16,1024]{1,0:T(8,128)(2,1)S(1)}, bf16[16,1024]{1,0:T(8,128)(2,1)}, u32[]{:S(2)}) copy-start(bf16[16,1024]{1,0:T(8,128)(2,1)} %param.12) | copy-start | bytes 98308
  7.2 4.1 %copy-start.2 = (bf16[2,1024,512]{2,1,0:T(8,128)(2,1)S(1)}, bf16[2,1024,512]{2,1,0:T(8,128)(2,1)}, u32[]{:S(2)}) copy-start(bf16[2,1024,512]{2,1,0:T(8,128)(2,1)} %param.17) | copy-start | bytes 6291460
  7.2 43.3 %all-reduce.11.cloned.1.call-start = ((), (), s32[]{:S(2)}) async-start(), calls=%async_computation.2 | async-start | bytes 393216
  8.1 5.0 %copy-start.4 = (bf16[2,1024,512]{2,1,0:T(8,128)(2,1)S(1)}, bf16[2,1024,512]{2,1,0:T(8,128)(2,1)}, u32[]{:S(2)}) copy-start(bf16[2,1024,512]{2,1,0:T(8,128)(2,1)} %param.19) | copy-start | bytes 6291460
  11.2 12.9 %copy-start.8 = (bf16[2,512]{1,0:T(2,128)(2,1)S(1)}, bf16[2,512]{1,0:T(2,128)(2,1)}, u32[]{:S(2)}) copy-start(bf16[2,512]{1,0:T(2,128)(2,1)} %param.23) | copy-start | bytes 6148
  11.2 12.9 %copy-start.9 = (f32[2,512]{1,0:T(2,128)S(1)}, f32[2,512]{1,0:T(2,128)}, u32[]{:S(2)}) copy-start(f32[2,512]{1,0:T(2,128)} %param.22) | copy-start | bytes 12292
  11.5 12.9 %copy-start.10 = (u32[32]{0:T(128)S(1)}, u32[32]{0:T(128)}, u32[]{:S(2)}) copy-start(u32[32]{0:T(128)} %constant.34) | copy-start | bytes 388
  11.5 40.2 %copy-start = (f32[2,4,8,64,64]{4,3,2,1,0:T(8,128)S(1)}, f32[2,4,8,64,64]{4,3,2,1,0:T(8,128)}, u32[]{:S(2)}) copy-start(f32[2,4,8,64,64]{4,3,2,1,0:T(8,128)} %param.13) | copy-start | bytes 3145732
  14.9 0.7 copy-start.6
  15.6 82.2 %all-reduce.7.cloned.1.call-start = ((), (), s32[]{:S(2)}) async-start(), calls=%async_computation | async-start | bytes 131072 | tf_op jit(solution)/shard_map/psum | solution.py:55
  63.3 80.5 %all-reduce.13.cloned.1.call-start = ((), (), s32[]{:S(2)}) async-start(), calls=%async_computation.3 | async-start | bytes 393216
  104.4 3.1 %copy-start.3 = (bf16[2,1024,512]{2,1,0:T(8,128)(2,1)S(1)}, bf16[2,1024,512]{2,1,0:T(8,128)(2,1)}, u32[]{:S(2)}) copy-start(bf16[2,1024,512]{2,1,0:T(8,128)(2,1)} %param.17) | copy-start | bytes 6291460
  104.4 4.8 %copy-start.5 = (bf16[2,1024,512]{2,1,0:T(8,128)(2,1)S(1)}, bf16[2,1024,512]{2,1,0:T(8,128)(2,1)}, u32[]{:S(2)}) copy-start(bf16[2,1024,512]{2,1,0:T(8,128)(2,1)} %param.19) | copy-start | bytes 6291460
  111.0 0.7 copy-start.7
  111.7 81.6 %all-reduce.9.cloned.1.call-start = ((), (), s32[]{:S(2)}) async-start(), calls=%async_computation.1 | async-start | bytes 131072 | tf_op jit(solution)/shard_map/psum | solution.py:55
Sparse Core Ops, SparseCore 0:
  15.7 34.7 all-reduce.10
  63.5 34.3 all-reduce.6
  111.8 31.9 all-reduce.12
  159.0 34.2 all-reduce.8
where the time goes:
time: 202 us; the launch traced here: 201 us
  waiting for transfers between devices  123 us (61%)
  matrix products  25.1 us (12%)
  blocking collectives  24.5 us (12%)
  between operations  14.5 us (7%)
  other arithmetic  11.5 us (6%)
  local copies, waits for them, and re-layouts  2.74 us (1%)
    psum x2, waiting for transfers between devices, run_block(): branch = lax.psum(branch_part, 'tp')  66 us
    unnamed x6, waiting for transfers between devices  56.8 us
    psum x2, blocking collectives, run_block(): all_totals = lax.psum(squares, 'dp')  14.1 us
    dot_general x12, matrix products, run_block(): jnp.dot(normed, weight, preferred_element_type=jnp.float32)  13.3 us
    all_gather x2, blocking collectives, run_block(): lax.all_gather(mixed, 'dp', axis=0, tiled=True)  10.4 us
    dot_general x2, matrix products, run_block(): jnp.dot(lax.all_gather(mixed, 'dp', axis=0, tiled=True), out_weight, pref...  4.2 us
    dot_general x2, matrix products, run_block(): jnp.einsum('bhij,bhj->bhi', new_state, recept, precision=lax.Precision.HI...  4.16 us
  transfers between devices with their start and end apart: 4, of which 4 were waited for; matrix products, arithmetic and copies ran while one was open for 2% of the time, Pallas kernels for 0%

commit v1 on v0

v1 whole, which is shorter than its diff:
```python
import functools

import jax
import jax.numpy as jnp
from jax import lax
from jax.experimental import pallas as pl
from jax.experimental.pallas import tpu as pltpu
from jax.sharding import PartitionSpec as P

F32 = jnp.float32
BF16 = jnp.bfloat16
MESH = pl.DeviceIdType.MESH
LANES = 128
ROLES = 6
KEY, RECEPT, DECAY, RATE, VALUE, GATE = range(ROLES)
PAIRS = ROLES // 2


def split2(x):
    high = x.astype(BF16).astype(F32)
    return jnp.concatenate([high, x - high], axis=0)


def kernel(
    n_dp, n_tp, width_all,
    stream, states, gain, rw, kw, vw, dw, tw, gw, ow, bias, hgain,
    out_stream, out_states,
    st_v, s_v, so_v, sb_v, gain_v, w_v, ow_v, bias_v, hgain_v, fin_v,
    proj_s, proj_r, sq_s, sq_r, mix_s, mix_r, br_s, br_r,
    small_sem, w_sem, ow_sem, s_sem, so_sem, fin_sem,
    pj_ss, pj_rs, sq_ss, sq_rs, mx_ss, mx_rs, br_ss, br_rs,
):
    dp = lax.axis_index("dp")
    tp = lax.axis_index("tp")
    seqs, cols = stream.shape
    layers, local, heads, head, _ = states.shape
    width = heads * head
    groups = width // LANES
    rows = groups * local

    small = [
        pltpu.make_async_copy(src, dst, small_sem.at[i])
        for i, (src, dst) in enumerate(
            [(stream, st_v), (gain, gain_v), (bias, bias_v), (hgain, hgain_v)]
        )
    ]
    weights = (kw, rw, dw, tw, vw, gw)
    w_copy = [
        [pltpu.make_async_copy(weights[r].at[l], w_v.at[l, r], w_sem.at[l, r]) for r in range(ROLES)]
        for l in range(layers)
    ]
    ow_copy = [pltpu.make_async_copy(ow.at[l], ow_v.at[l], ow_sem.at[l]) for l in range(layers)]
    s_copy = [pltpu.make_async_copy(states.at[l], s_v.at[l], s_sem.at[l]) for l in range(layers)]
    for copy in small:
        copy.start()
    for copy in w_copy[0]:
        copy.start()

    barrier = pltpu.get_barrier_semaphore()
    for k in range(1, n_dp):
        pl.semaphore_signal(barrier, inc=1, device_id={"dp": lax.rem(dp + k, n_dp)}, device_id_type=MESH)
    for k in range(1, n_tp):
        pl.semaphore_signal(barrier, inc=1, device_id={"tp": lax.rem(tp + k, n_tp)}, device_id_type=MESH)

    lane_r = lax.broadcasted_iota(jnp.int32, (LANES, LANES), 0)
    lane_c = lax.broadcasted_iota(jnp.int32, (LANES, LANES), 1)
    same_head = jnp.where((lane_r < head) == (lane_c < head), 1.0, 0.0).astype(BF16)

    def head_sum(x):
        both = jnp.dot(split2(x).astype(BF16), same_head, preferred_element_type=F32)
        return both[: x.shape[0]] + both[x.shape[0]:]

    first_head = lax.broadcasted_iota(jnp.int32, (2 * rows, LANES), 1) < head
    pair_row = lax.broadcasted_iota(jnp.int32, (2 * rows, LANES), 0)

    def fold(row):
        return jnp.concatenate(
            [jnp.broadcast_to(row[:, g * LANES:(g + 1) * LANES], (local, LANES)) for g in range(groups)], axis=0
        )

    started = []
    for copy in small:
        copy.wait()
    current = st_v[...].astype(F32)
    for l in range(layers):
        square = jnp.sum(current * current, axis=1, keepdims=True)
        normed = (current * gain_v[l:l + 1, :].astype(F32)).astype(BF16)
        wide = jnp.broadcast_to(square, (seqs, LANES))
        for d in range(n_dp):
            sq_s[l, d] = wide[d * local:(d + 1) * local]

        def send(src, dst, ss, rs, axis, index, size):
            for k in range(1, size):
                peer = lax.rem(index + k, size)
                copy = pltpu.make_async_remote_copy(
                    src_ref=src(peer), dst_ref=dst(index), send_sem=ss.at[k], recv_sem=rs.at[index],
                    device_id={axis: peer}, device_id_type=MESH,
                )
                copy.start()
                started.append(copy)

        def receive(src, dst, ss, rs, axis, index, size):
            for k in range(1, size):
                peer = lax.rem(index + k, size)
                pltpu.make_async_remote_copy(
                    src_ref=src(peer), dst_ref=dst(peer), send_sem=ss.at[k], recv_sem=rs.at[peer],
                    device_id={axis: peer}, device_id_type=MESH,
                ).wait_recv()

        sq_args = (
            lambda p: sq_s.at[l, p], lambda p: sq_r.at[l, p], sq_ss.at[l], sq_rs.at[l], "dp", dp, n_dp,
        )
        pj_args = [
            (
                lambda p, c=c: proj_s.at[l, c, p], lambda p, c=c: proj_r.at[l, c, p],
                pj_ss.at[l, c], pj_rs.at[l, c], "dp", dp, n_dp,
            )
            for c in range(PAIRS)
        ]
        for r in range(ROLES):
            w_copy[l][r].wait()
            value = jnp.dot(normed, w_v[l, r], preferred_element_type=F32)
            for d in range(n_dp):
                block = value[d * local:(d + 1) * local]
                proj_s[l, r // 2, d, r % 2] = jnp.concatenate(
                    [block[:, g * LANES:(g + 1) * LANES] for g in range(groups)], axis=0
                ).astype(BF16)
            if r % 2 == 1:
                if l == 0 and r == 1:
                    pl.semaphore_wait(barrier, n_dp - 1 + n_tp - 1)
                if r == 1:
                    send(*sq_args)
                send(*pj_args[r // 2])
        if l == 0:
            s_copy[0].start()
            ow_copy[0].start()
            for copy in w_copy[1]:
                copy.start()
            s_copy[1].start()
            ow_copy[1].start()

        s_copy[l].wait()
        for q in range(local):
            sb_v[l, q] = s_v[l, q].reshape(width, head).astype(BF16)

        receive(*sq_args)
        total = sq_s[l, dp]
        for k in range(1, n_dp):
            total = total + sq_r[l, lax.rem(dp + k, n_dp)]
        inv_rms = lax.rsqrt(total / width_all + 1e-06)
        inv_rms = jnp.concatenate([inv_rms] * groups, axis=0)

        roles = []
        for c in range(PAIRS):
            receive(*pj_args[c])
            for half in range(2):
                acc = proj_s[l, c, dp, half].astype(F32)
                for k in range(1, n_dp):
                    acc = acc + proj_r[l, c, lax.rem(dp + k, n_dp), half].astype(F32)
                roles.append(acc * inv_rms)
        key, recept, decay_pre, rate_pre, val, gate_pre = roles

        decay = jnp.exp(-0.606531 * jax.nn.sigmoid(fold(bias_v[l:l + 1, :]) + decay_pre))
        rate = jax.nn.sigmoid(rate_pre)
        vectors = split2(jnp.concatenate([key, decay * recept], axis=0))
        lhs = jnp.concatenate([vectors[:, :head], vectors[:, head:]], axis=0).astype(BF16)
        found = jnp.zeros((2 * rows, LANES), F32)
        for q in range(local):
            prod = lax.dot_general(lhs, sb_v[l, q], (((1,), (1,)), ((), ())), preferred_element_type=F32)
            first = prod[:2 * rows] + prod[2 * rows:4 * rows]
            second = prod[4 * rows:6 * rows] + prod[6 * rows:]
            for g in range(groups):
                at = g * local + q
                lanes = slice(g * LANES, (g + 1) * LANES)
                mine = (pair_row == at) | (pair_row == rows + at)
                found = jnp.where(mine, jnp.where(first_head, first[:, lanes], second[:, lanes]), found)

        sums = head_sum(jnp.concatenate([key * key, key * rate * recept, key * recept], axis=0))
        inv_norm = lax.rsqrt(sums[:rows] + 1e-06)
        removed = found[:rows] * inv_norm
        key_rate = key * rate * inv_norm
        read = found[rows:] - removed * (sums[rows:2 * rows] * inv_norm) + val * sums[2 * rows:]
        center = read - head_sum(read) / head
        normal = center * lax.rsqrt(head_sum(center * center) / head + 1e-05)
        mixed = normal * fold(hgain_v[l:l + 1, :].astype(F32)) * jax.nn.sigmoid(gate_pre)
        mix_s[l] = mixed.astype(BF16)
        mx_args = (lambda p: mix_s.at[l], lambda p: mix_r.at[l, p], mx_ss.at[l], mx_rs.at[l], "dp", dp, n_dp)
        send(*mx_args)
        mix_r[l, dp] = mix_s[l]

        tall = jnp.concatenate([removed, val, jnp.zeros((LANES - 2 * rows, LANES), F32)], axis=0)
        tall = jnp.transpose(tall)
        halves = [[x[:, half * head:(half + 1) * head] for x in (decay, key_rate, key)] for half in range(2)]
        for g in range(groups):
            for q in range(local):
                at = g * local + q
                for half in range(2):
                    h = 2 * g + half
                    d_row, r_row, k_row = [x[at:at + 1] for x in halves[half]]
                    part = tall[half * head:(half + 1) * head]
                    so_v[l, q, h] = (
                        s_v[l, q, h] * d_row - part[:, at:at + 1] * r_row + part[:, rows + at:rows + at + 1] * k_row
                    )
        so_copy = pltpu.make_async_copy(so_v.at[l], out_states.at[l], so_sem.at[l])
        so_copy.start()

        ow_copy[l].wait()
        receive(*mx_args)
        blocks = [mix_r[l, s].astype(F32) for s in range(n_dp)]
        gathered = jnp.concatenate(
            [
                jnp.concatenate([b[g * local:(g + 1) * local] for b in blocks], axis=0)
                for g in range(groups)
            ],
            axis=1,
        ).astype(BF16)
        br_s[l] = jnp.dot(gathered, ow_v[l], preferred_element_type=F32).astype(BF16)
        br_args = (lambda p: br_s.at[l], lambda p: br_r.at[l, p], br_ss.at[l], br_rs.at[l], "tp", tp, n_tp)
        send(*br_args)
        br_r[l, tp] = br_s[l]
        receive(*br_args)
        branch = br_r[l, 0].astype(F32)
        for s in range(1, n_tp):
            branch = branch + br_r[l, s].astype(F32)
        rounded = (current + branch).astype(BF16)
        current = rounded.astype(F32)
        if l == layers - 1:
            fin_v[...] = rounded
            fin = pltpu.make_async_copy(fin_v, out_stream, fin_sem)
            fin.start()
            fin.wait()

    for copy in started:
        copy.wait_send()
    for l in range(layers):
        pltpu.make_async_copy(so_v.at[l], out_states.at[l], so_sem.at[l]).wait()


def solution(mesh):
    n_dp, n_tp = mesh.shape["dp"], mesh.shape["tp"]

    def per_device(stream, states, gain, rw, kw, vw, dw, tw, gw, ow, bias, hgain):
        seqs, cols = stream.shape
        layers, local, heads, head, _ = states.shape
        width = heads * head
        rows = width // LANES * local
        dma = pltpu.SemaphoreType.DMA
        any_spec = pl.BlockSpec(memory_space=pl.ANY)
        return pl.pallas_call(
            functools.partial(kernel, n_dp, n_tp, cols * n_dp),
            out_shape=(
                jax.ShapeDtypeStruct(stream.shape, BF16),
                jax.ShapeDtypeStruct(states.shape, F32),
            ),
            in_specs=[any_spec] * 12,
            out_specs=(any_spec, any_spec),
            scratch_shapes=[
                pltpu.VMEM(stream.shape, BF16),
                pltpu.VMEM(states.shape, F32),
                pltpu.VMEM(states.shape, F32),
                pltpu.VMEM((layers, local, width, head), BF16),
                pltpu.VMEM(gain.shape, BF16),
                pltpu.VMEM((layers, ROLES, cols, width), BF16),
                pltpu.VMEM(ow.shape, BF16),
                pltpu.VMEM(bias.shape, F32),
                pltpu.VMEM(hgain.shape, BF16),
                pltpu.VMEM(stream.shape, BF16),
                pltpu.VMEM((layers, PAIRS, n_dp, 2, rows, LANES), BF16),
                pltpu.VMEM((layers, PAIRS, n_dp, 2, rows, LANES), BF16),
                pltpu.VMEM((layers, n_dp, local, LANES), F32),
                pltpu.VMEM((layers, n_dp, local, LANES), F32),
                pltpu.VMEM((layers, rows, LANES), BF16),
                pltpu.VMEM((layers, n_dp, rows, LANES), BF16),
                pltpu.VMEM((layers, seqs, cols), BF16),
                pltpu.VMEM((layers, n_tp, seqs, cols), BF16),
                dma((4,)),
                dma((layers, ROLES)),
                dma((layers,)),
                dma((layers,)),
                dma((layers,)),
                dma,
                dma((layers, PAIRS, n_dp)),
                dma((layers, PAIRS, n_dp)),
                dma((layers, n_dp)),
                dma((layers, n_dp)),
                dma((layers, n_dp)),
                dma((layers, n_dp)),
                dma((layers, n_tp)),
                dma((layers, n_tp)),
            ],
            compiler_params=pltpu.CompilerParams(
                collective_id=0, has_side_effects=True, vmem_limit_bytes=60 * 1024 * 1024
            ),
            name="two_blocks",
        )(stream, states, gain, rw, kw, vw, dw, tw, gw, ow, bias, hgain)

    in_specs = (
        P("grp", "dp"),
        P(None, ("grp", "dp"), "tp", None, None),
        P(None, "dp"),
        P(None, "dp", "tp"),
        P(None, "dp", "tp"),
        P(None, "dp", "tp"),
        P(None, "dp", "tp"),
        P(None, "dp", "tp"),
        P(None, "dp", "tp"),
        P(None, "tp", "dp"),
        P(None, "tp"),
        P(None, "tp"),
    )
    out_specs = (P("grp", "dp"), P(None, ("grp", "dp"), "tp", None, None))
    return jax.shard_map(
        per_device, mesh=mesh, in_specs=in_specs, out_specs=out_specs, check_vma=False
    )
```

time: 202 us -> 37.5 us (0.19)
  waiting for transfers between devices: 123 us -> 0 us
  Pallas kernels: 0 us -> 32.2 us
  matrix products: 25.1 us -> 0 us
  blocking collectives: 24.5 us -> 0 us
  between operations: 14.5 us -> 0.64 us
  other arithmetic: 11.5 us -> 0 us
    psum x2 -> x0, waiting for transfers between devices: 66 us -> none  [run_block(): branch = lax.psum(branch_part, 'tp')]
    unnamed x6 -> x0, waiting for transfers between devices: 56.8 us -> none
    pallas_call x0 -> x1, Pallas kernels: none -> 32.2 us  [per_device(): pl.pallas_call(functools.partial(kernel, n_dp, n_tp, cols * n_dp), out_sh...]
    dot_general x18 -> x0, matrix products: 25.1 us -> none  [the longest x12 13.3 us: run_block(): jnp.dot(normed, weight, preferred_element_type=jnp.float32)]
    psum x2 -> x0, blocking collectives: 14.1 us -> none  [run_block(): all_totals = lax.psum(squares, 'dp')]
    all_gather x2 -> x0, blocking collectives: 10.4 us -> none  [run_block(): lax.all_gather(mixed, 'dp', axis=0, tiled=True)]
    mul x5 -> x0, other arithmetic: 2.95 us -> none  [the longest x2 1.93 us: run_block(): projected = (summed * inv_rms).reshape(local_rows, 6, -1, HEAD)]
    another operation x1 -> x0, other arithmetic: 2.76 us -> none  [per_device(): return (current, jnp.stack(fresh_list))]
  transfers between devices with their start and end apart: 4 -> 0, of which waited for: 4 -> 0; matrix products, arithmetic and copies ran while one was open for 2% -> 0% of each run, Pallas kernels for 0% -> 0%
where the time goes in v1:
time: 37.5 us; the launch traced here: 37.3 us
  Pallas kernels  32.2 us (86%)
  local copies, waits for them, and re-layouts  4.53 us (12%)
  between operations  0.64 us (2%)
    pallas_call x1, Pallas kernels, per_device(): pl.pallas_call(functools.partial(kernel, n_dp, n_tp, cols * n_dp), out_sh...  32.2 us
    unnamed x2, local copies, waits for them, and re-layouts  4.53 us

profile of v1, /device:TPU:0, one launch (start us, length us, event | category | flops | bytes accessed | tf_op | source)
XLA Modules:
  0.0 37.3 jit_solution(14316771439421405742)
XLA Ops:
  0.6 32.2 %two_blocks.1 = (bf16[16,1024]{1,0:T(8,128)(2,1)}, f32[2,4,8,64,64]{4,3,2,1,0:T(8,128)}) custom-call(bf16[16,1024]{1,0:T(8,128)(2,1)} %stream.1, f32[2,4,8,64,64]{4,3,2,1,0:T(8,128)} %states.1, bf16[2,1024]{1,0:T(2,128)(2,1)} %gain.1, bf16[2,1024,512]{2,1,0:T(8,128)(2,1)} %rw.1, bf16[2,1024,512]{2,1,0:T(8,128)(2,1)} %kw.1, bf16[2,1024,512]{2,1,0:T(8,128)(2,1)} %vw.1, ...), custom_call_target="tpu_custom_call" | custom-call | tf_op jit(solution)/shard_map/two_blocks/pallas_call | solution.py:249
  32.8 1.4 %copy.16 = bf16[16,1024]{1,0:T(8,128)(2,1)} copy(bf16[16,1024]{1,0:T(8,128)(2,1)} %get-tuple-element.4) | data formatting | bytes 65536
  34.2 3.2 %copy.17 = f32[2,4,8,64,64]{4,3,2,1,0:T(8,128)} copy(f32[2,4,8,64,64]{4,3,2,1,0:T(8,128)} %get-tuple-element.5) | data formatting | bytes 2097152

commit v2 on v1

--- a/solution.py
+++ b/solution.py
@@ -25,9 +25,9 @@
     n_dp, n_tp, width_all,
     stream, states, gain, rw, kw, vw, dw, tw, gw, ow, bias, hgain,
     out_stream, out_states,
-    st_v, s_v, so_v, sb_v, gain_v, w_v, ow_v, bias_v, hgain_v, fin_v,
+    st_v, s_v, sb_v, gain_v, w_v, ow_v, bias_v, hgain_v,
     proj_s, proj_r, sq_s, sq_r, mix_s, mix_r, br_s, br_r,
-    small_sem, w_sem, ow_sem, s_sem, so_sem, fin_sem,
+    small_sem, w_sem, ow_sem, s_sem,
     pj_ss, pj_rs, sq_ss, sq_rs, mx_ss, mx_rs, br_ss, br_rs,
 ):
     dp = lax.axis_index("dp")
@@ -55,6 +55,7 @@
         copy.start()
     for copy in w_copy[0]:
         copy.start()
+    s_copy[0].start()
 
     barrier = pltpu.get_barrier_semaphore()
     for k in range(1, n_dp):
@@ -79,7 +80,7 @@
         )
 
     started = []
-    for copy in small:
+    for copy in small[:2]:
         copy.wait()
     current = st_v[...].astype(F32)
     for l in range(layers):
@@ -125,23 +126,27 @@
                 proj_s[l, r // 2, d, r % 2] = jnp.concatenate(
                     [block[:, g * LANES:(g + 1) * LANES] for g in range(groups)], axis=0
                 ).astype(BF16)
-            if r % 2 == 1:
-                if l == 0 and r == 1:
-                    pl.semaphore_wait(barrier, n_dp - 1 + n_tp - 1)
+            if l > 0 and r % 2 == 1:
                 if r == 1:
                     send(*sq_args)
                 send(*pj_args[r // 2])
         if l == 0:
-            s_copy[0].start()
-            ow_copy[0].start()
-            for copy in w_copy[1]:
-                copy.start()
-            s_copy[1].start()
-            ow_copy[1].start()
-
+            pl.semaphore_wait(barrier, n_dp - 1 + n_tp - 1)
+            send(*sq_args)
+            for c in range(PAIRS):
+                send(*pj_args[c])
+            for copy in small[2:]:
+                copy.wait()
         s_copy[l].wait()
         for q in range(local):
             sb_v[l, q] = s_v[l, q].reshape(width, head).astype(BF16)
+        if l == 0:
+            ow_copy[0].start()
+            for later in range(1, layers):
+                for copy in w_copy[later]:
+                    copy.start()
+                s_copy[later].start()
+                ow_copy[later].start()
 
         receive(*sq_args)
         total = sq_s[l, dp]
@@ -150,15 +155,16 @@
         inv_rms = lax.rsqrt(total / width_all + 1e-06)
         inv_rms = jnp.concatenate([inv_rms] * groups, axis=0)
 
-        roles = []
-        for c in range(PAIRS):
+        def projected(c):
             receive(*pj_args[c])
             for half in range(2):
                 acc = proj_s[l, c, dp, half].astype(F32)
                 for k in range(1, n_dp):
                     acc = acc + proj_r[l, c, lax.rem(dp + k, n_dp), half].astype(F32)
-                roles.append(acc * inv_rms)
-        key, recept, decay_pre, rate_pre, val, gate_pre = roles
+                yield acc * inv_rms
+
+        key, recept = projected(0)
+        decay_pre, rate_pre = projected(1)
 
         decay = jnp.exp(-0.606531 * jax.nn.sigmoid(fold(bias_v[l:l + 1, :]) + decay_pre))
         rate = jax.nn.sigmoid(rate_pre)
@@ -179,6 +185,7 @@
         inv_norm = lax.rsqrt(sums[:rows] + 1e-06)
         removed = found[:rows] * inv_norm
         key_rate = key * rate * inv_norm
+        val, gate_pre = projected(2)
         read = found[rows:] - removed * (sums[rows:2 * rows] * inv_norm) + val * sums[2 * rows:]
         center = read - head_sum(read) / head
         normal = center * lax.rsqrt(head_sum(center * center) / head + 1e-05)
@@ -191,18 +198,19 @@
         tall = jnp.concatenate([removed, val, jnp.zeros((LANES - 2 * rows, LANES), F32)], axis=0)
         tall = jnp.transpose(tall)
         halves = [[x[:, half * head:(half + 1) * head] for x in (decay, key_rate, key)] for half in range(2)]
-        for g in range(groups):
-            for q in range(local):
-                at = g * local + q
+
+        def renew(first_row, last_row):
+            for at in range(first_row, last_row):
+                g, q = at // local, at % local
                 for half in range(2):
                     h = 2 * g + half
                     d_row, r_row, k_row = [x[at:at + 1] for x in halves[half]]
                     part = tall[half * head:(half + 1) * head]
-                    so_v[l, q, h] = (
+                    out_states[l, q, h] = (
                         s_v[l, q, h] * d_row - part[:, at:at + 1] * r_row + part[:, rows + at:rows + at + 1] * k_row
                     )
-        so_copy = pltpu.make_async_copy(so_v.at[l], out_states.at[l], so_sem.at[l])
-        so_copy.start()
+
+        renew(0, rows // 2)
 
         ow_copy[l].wait()
         receive(*mx_args)
@@ -218,6 +226,7 @@
         br_args = (lambda p: br_s.at[l], lambda p: br_r.at[l, p], br_ss.at[l], br_rs.at[l], "tp", tp, n_tp)
         send(*br_args)
         br_r[l, tp] = br_s[l]
+        renew(rows // 2, rows)
         receive(*br_args)
         branch = br_r[l, 0].astype(F32)
         for s in range(1, n_tp):
@@ -225,15 +234,10 @@
         rounded = (current + branch).astype(BF16)
         current = rounded.astype(F32)
         if l == layers - 1:
-            fin_v[...] = rounded
-            fin = pltpu.make_async_copy(fin_v, out_stream, fin_sem)
-            fin.start()
-            fin.wait()
+            out_stream[...] = rounded
 
     for copy in started:
         copy.wait_send()
-    for l in range(layers):
-        pltpu.make_async_copy(so_v.at[l], out_states.at[l], so_sem.at[l]).wait()
 
 
 def solution(mesh):
@@ -245,18 +249,17 @@
         width = heads * head
         rows = width // LANES * local
         dma = pltpu.SemaphoreType.DMA
-        any_spec = pl.BlockSpec(memory_space=pl.ANY)
+        hbm_spec = pl.BlockSpec(memory_space=pltpu.HBM)
         return pl.pallas_call(
             functools.partial(kernel, n_dp, n_tp, cols * n_dp),
             out_shape=(
-                jax.ShapeDtypeStruct(stream.shape, BF16),
-                jax.ShapeDtypeStruct(states.shape, F32),
+                pltpu.VMEM(stream.shape, BF16),
+                pltpu.VMEM(states.shape, F32),
             ),
-            in_specs=[any_spec] * 12,
-            out_specs=(any_spec, any_spec),
+            in_specs=[hbm_spec] * 12,
+            out_specs=(pl.BlockSpec(memory_space=pltpu.VMEM),) * 2,
             scratch_shapes=[
                 pltpu.VMEM(stream.shape, BF16),
-                pltpu.VMEM(states.shape, F32),
                 pltpu.VMEM(states.shape, F32),
                 pltpu.VMEM((layers, local, width, head), BF16),
                 pltpu.VMEM(gain.shape, BF16),
@@ -264,7 +267,6 @@
                 pltpu.VMEM(ow.shape, BF16),
                 pltpu.VMEM(bias.shape, F32),
                 pltpu.VMEM(hgain.shape, BF16),
-                pltpu.VMEM(stream.shape, BF16),
                 pltpu.VMEM((layers, PAIRS, n_dp, 2, rows, LANES), BF16),
                 pltpu.VMEM((layers, PAIRS, n_dp, 2, rows, LANES), BF16),
                 pltpu.VMEM((layers, n_dp, local, LANES), F32),
@@ -277,8 +279,6 @@
                 dma((layers, ROLES)),
                 dma((layers,)),
                 dma((layers,)),
-                dma((layers,)),
-                dma,
                 dma((layers, PAIRS, n_dp)),
                 dma((layers, PAIRS, n_dp)),
                 dma((layers, n_dp)),
@@ -289,7 +289,7 @@
                 dma((layers, n_tp)),
             ],
             compiler_params=pltpu.CompilerParams(
-                collective_id=0, has_side_effects=True, vmem_limit_bytes=60 * 1024 * 1024
+                collective_id=0, has_side_effects=True, vmem_limit_bytes=56 * 1024 * 1024
             ),
             name="two_blocks",
         )(stream, states, gain, rw, kw, vw, dw, tw, gw, ow, bias, hgain)

time: 37.5 us -> 33 us (0.88)
  local copies, waits for them, and re-layouts: 4.53 us -> 1.94 us
  Pallas kernels: 32.2 us -> 30.3 us
    unnamed x2, local copies, waits for them, and re-layouts: 4.53 us -> 1.94 us
    pallas_call x1, Pallas kernels: 32.2 us -> 30.3 us  [per_device(): pl.pallas_call(functools.partial(kernel, n_dp, n_tp, cols * n_dp), out_sh...]
where the time goes in v2:
time: 33 us; the launch traced here: 32.9 us
  Pallas kernels  30.3 us (92%)
  local copies, waits for them, and re-layouts  1.94 us (6%)
  between operations  0.64 us (2%)
    pallas_call x1, Pallas kernels, per_device(): pl.pallas_call(functools.partial(kernel, n_dp, n_tp, cols * n_dp), out_sh...  30.3 us
    unnamed x2, local copies, waits for them, and re-layouts  1.94 us

profile of v2, /device:TPU:0, one launch (start us, length us, event | category | flops | bytes accessed | tf_op | source)
XLA Modules:
  0.0 32.9 jit_solution(7738062541460635257)
XLA Ops:
  0.6 30.3 %two_blocks.1 = (bf16[16,1024]{1,0:T(8,128)(2,1)S(1)}, f32[2,4,8,64,64]{4,3,2,1,0:T(8,128)S(1)}) custom-call(bf16[16,1024]{1,0:T(8,128)(2,1)} %stream.1, f32[2,4,8,64,64]{4,3,2,1,0:T(8,128)} %states.1, bf16[2,1024]{1,0:T(2,128)(2,1)} %gain.1, bf16[2,1024,512]{2,1,0:T(8,128)(2,1)} %rw.1, bf16[2,1024,512]{2,1,0:T(8,128)(2,1)} %kw.1, bf16[2,1024,512]{2,1,0:T(8,128)(2,1)} %vw.1, ...), custom_call_target="tpu_custom_call" | custom-call | tf_op jit(solution)/shard_map/two_blocks/pallas_call | solution.py:253
  30.9 0.6 %copy.16 = bf16[16,1024]{1,0:T(8,128)(2,1)} copy(bf16[16,1024]{1,0:T(8,128)(2,1)S(1)} %get-tuple-element.2) | data formatting | bytes 65536
  31.6 1.3 %copy.17 = f32[2,4,8,64,64]{4,3,2,1,0:T(8,128)} copy(f32[2,4,8,64,64]{4,3,2,1,0:T(8,128)S(1)} %get-tuple-element.3) | data formatting | bytes 2097152

commit v3 on v2

--- a/solution.py
+++ b/solution.py
@@ -82,17 +82,25 @@
     started = []
     for copy in small[:2]:
         copy.wait()
-    current = st_v[...].astype(F32)
+    chunks = br_s.shape[1]
+    part_cols = cols // chunks
+    spans = [slice(c * part_cols, (c + 1) * part_cols) for c in range(chunks)]
+    current = [st_v[:, span].astype(F32) for span in spans]
     for l in range(layers):
-        square = jnp.sum(current * current, axis=1, keepdims=True)
-        normed = (current * gain_v[l:l + 1, :].astype(F32)).astype(BF16)
-        wide = jnp.broadcast_to(square, (seqs, LANES))
-        for d in range(n_dp):
-            sq_s[l, d] = wide[d * local:(d + 1) * local]
+
+        def norm(c):
+            x = current[c]
+            square = jnp.sum(x * x, axis=1, keepdims=True)
+            return square, (x * gain_v[l:l + 1, spans[c]].astype(F32)).astype(BF16)
 
         def send(src, dst, ss, rs, axis, index, size):
             for k in range(1, size):
                 peer = lax.rem(index + k, size)
+                if axis == "tp":
+                    down, up = size - k, k - 1
+                    down = jnp.where(down > index, down, down - 1)
+                    up = jnp.where(up < index, up, up + 1)
+                    peer = jnp.where(2 * index < size, down, up)
                 copy = pltpu.make_async_remote_copy(
                     src_ref=src(peer), dst_ref=dst(index), send_sem=ss.at[k], recv_sem=rs.at[index],
                     device_id={axis: peer}, device_id_type=MESH,
@@ -118,23 +126,50 @@
             )
             for c in range(PAIRS)
         ]
+        parts = []
+        if l == 0:
+            squares, normed = zip(*[norm(c) for c in range(chunks)])
+            square, last = sum(squares), jnp.concatenate(normed, axis=1)
+            last_span = slice(0, cols)
+        else:
+            square = 0.0
+            for c in range(chunks):
+                current[c] = arrive(c)
+                more, last = norm(c)
+                square = square + more
+                last_span = spans[c]
+                if c < chunks - 1:
+                    for r in range(ROLES):
+                        if c == 0:
+                            w_copy[l][r].wait()
+                        value = jnp.dot(last, w_v[l, r, last_span], preferred_element_type=F32)
+                        if c == 0:
+                            parts.append(value)
+                        else:
+                            parts[r] = parts[r] + value
+        wide = jnp.broadcast_to(square, (seqs, LANES))
+        for d in range(n_dp):
+            sq_s[l, d] = wide[d * local:(d + 1) * local]
+        if l > 0:
+            send(*sq_args)
         for r in range(ROLES):
-            w_copy[l][r].wait()
-            value = jnp.dot(normed, w_v[l, r], preferred_element_type=F32)
+            if not parts:
+                w_copy[l][r].wait()
+            value = jnp.dot(last, w_v[l, r, last_span], preferred_element_type=F32)
+            if parts:
+                value = value + parts[r]
             for d in range(n_dp):
                 block = value[d * local:(d + 1) * local]
                 proj_s[l, r // 2, d, r % 2] = jnp.concatenate(
                     [block[:, g * LANES:(g + 1) * LANES] for g in range(groups)], axis=0
                 ).astype(BF16)
-            if l > 0 and r % 2 == 1:
-                if r == 1:
-                    send(*sq_args)
+            if l == 0 and r == 3:
+                pl.semaphore_wait(barrier, n_dp - 1 + n_tp - 1)
+                send(*sq_args)
+                send(*pj_args[0])
+            if r % 2 == 1 and (l > 0 or r > 1):
                 send(*pj_args[r // 2])
         if l == 0:
-            pl.semaphore_wait(barrier, n_dp - 1 + n_tp - 1)
-            send(*sq_args)
-            for c in range(PAIRS):
-                send(*pj_args[c])
             for copy in small[2:]:
                 copy.wait()
         s_copy[l].wait()
@@ -222,22 +257,45 @@
             ],
             axis=1,
         ).astype(BF16)
-        br_s[l] = jnp.dot(gathered, ow_v[l], preferred_element_type=F32).astype(BF16)
-        br_args = (lambda p: br_s.at[l], lambda p: br_r.at[l, p], br_ss.at[l], br_rs.at[l], "tp", tp, n_tp)
-        send(*br_args)
-        br_r[l, tp] = br_s[l]
+        br_args = [
+            (
+                lambda p, c=c: br_s.at[l, c], lambda p, c=c: br_r.at[l, p, c],
+                br_ss.at[l, c], br_rs.at[l, c], "tp", tp, n_tp,
+            )
+            for c in range(chunks)
+        ]
+        for c in range(chunks):
+            br_s[l, c] = jnp.dot(gathered, ow_v[l, :, spans[c]], preferred_element_type=F32).astype(BF16)
+            send(*br_args[c])
+        for c in range(chunks):
+            br_r[l, tp, c] = br_s[l, c]
         renew(rows // 2, rows)
-        receive(*br_args)
-        branch = br_r[l, 0].astype(F32)
-        for s in range(1, n_tp):
-            branch = branch + br_r[l, s].astype(F32)
-        rounded = (current + branch).astype(BF16)
-        current = rounded.astype(F32)
-        if l == layers - 1:
-            out_stream[...] = rounded
-
+
+        def arrive(c, l=l, receive=receive, br_args=br_args):
+            receive(*br_args[c])
+            branch = br_r[l, 0, c].astype(F32)
+            for s in range(1, n_tp):
+                branch = branch + br_r[l, s, c].astype(F32)
+            return (current[c] + branch).astype(BF16).astype(F32)
+
+    for c in range(chunks):
+        out_stream[:, spans[c]] = arrive(c).astype(BF16)
     for copy in started:
         copy.wait_send()
+
+
+def flush(stream, states, out_stream, out_states, sem):
+    copies = [pltpu.make_async_copy(stream, out_stream, sem.at[0])]
+    layers, local = states.shape[:2]
+    for l in range(layers):
+        for q in range(local):
+            copies.append(
+                pltpu.make_async_copy(states.at[l, q], out_states.at[l, q], sem.at[1 + l * local + q])
+            )
+    for copy in copies:
+        copy.start()
+    for copy in copies:
+        copy.wait()
 
 
 def solution(mesh):
@@ -248,9 +306,10 @@
         layers, local, heads, head, _ = states.shape
         width = heads * head
         rows = width // LANES * local
+        chunks = 2 if cols % (2 * LANES) == 0 else 1
         dma = pltpu.SemaphoreType.DMA
         hbm_spec = pl.BlockSpec(memory_space=pltpu.HBM)
-        return pl.pallas_call(
+        new_stream, new_states = pl.pallas_call(
             functools.partial(kernel, n_dp, n_tp, cols * n_dp),
             out_shape=(
                 pltpu.VMEM(stream.shape, BF16),
@@ -273,8 +332,8 @@
                 pltpu.VMEM((layers, n_dp, local, LANES), F32),
                 pltpu.VMEM((layers, rows, LANES), BF16),
                 pltpu.VMEM((layers, n_dp, rows, LANES), BF16),
-                pltpu.VMEM((layers, seqs, cols), BF16),
-                pltpu.VMEM((layers, n_tp, seqs, cols), BF16),
+                pltpu.VMEM((layers, chunks, seqs, cols // chunks), BF16),
+                pltpu.VMEM((layers, n_tp, chunks, seqs, cols // chunks), BF16),
                 dma((4,)),
                 dma((layers, ROLES)),
                 dma((layers,)),
@@ -285,14 +344,26 @@
                 dma((layers, n_dp)),
                 dma((layers, n_dp)),
                 dma((layers, n_dp)),
-                dma((layers, n_tp)),
-                dma((layers, n_tp)),
+                dma((layers, chunks, n_tp)),
+                dma((layers, chunks, n_tp)),
             ],
             compiler_params=pltpu.CompilerParams(
                 collective_id=0, has_side_effects=True, vmem_limit_bytes=56 * 1024 * 1024
             ),
             name="two_blocks",
         )(stream, states, gain, rw, kw, vw, dw, tw, gw, ow, bias, hgain)
+        return pl.pallas_call(
+            flush,
+            out_shape=(
+                jax.ShapeDtypeStruct(stream.shape, BF16),
+                jax.ShapeDtypeStruct(states.shape, F32),
+            ),
+            in_specs=[pl.BlockSpec(memory_space=pltpu.VMEM)] * 2,
+            out_specs=(hbm_spec,) * 2,
+            scratch_shapes=[dma((1 + layers * local,))],
+            compiler_params=pltpu.CompilerParams(vmem_limit_bytes=1024 * 1024),
+            name="flush",
+        )(new_stream, new_states)
 
     in_specs = (
         P("grp", "dp"),

time: 33 us -> 31.5 us (0.955)
  local copies, waits for them, and re-layouts: 1.94 us -> 0 us
  Pallas kernels: 30.3 us -> 30.7 us
    unnamed x2 -> x0, local copies, waits for them, and re-layouts: 1.94 us -> none
    pallas_call x0 -> x1, Pallas kernels: none -> 1.4 us  [per_device(): pl.pallas_call(flush, out_shape=(jax.ShapeDtypeStruct(stream.shape, BF16)...]
    pallas_call x1, Pallas kernels: 30.3 us -> 29.3 us  [per_device(): pl.pallas_call(functools.partial(kernel, n_dp, n_tp, cols * n_dp), out_sh...]
where the time goes in v3:
time: 31.5 us; the launch traced here: 31.3 us
  Pallas kernels  30.7 us (97%)
  between operations  0.64 us (2%)
    pallas_call x1, Pallas kernels, per_device(): pl.pallas_call(functools.partial(kernel, n_dp, n_tp, cols * n_dp), out_sh...  29.3 us
    pallas_call x1, Pallas kernels, per_device(): pl.pallas_call(flush, out_shape=(jax.ShapeDtypeStruct(stream.shape, BF16)...  1.4 us

profile of v3, /device:TPU:0, one launch (start us, length us, event | category | flops | bytes accessed | tf_op | source)
XLA Modules:
  0.0 31.3 jit_solution(6152402507744378225)
XLA Ops:
  0.6 29.3 %two_blocks.1 = (bf16[16,1024]{1,0:T(8,128)(2,1)S(1)}, f32[2,4,8,64,64]{4,3,2,1,0:T(8,128)S(1)}) custom-call(bf16[16,1024]{1,0:T(8,128)(2,1)} %stream.1, f32[2,4,8,64,64]{4,3,2,1,0:T(8,128)} %states.1, bf16[2,1024]{1,0:T(2,128)(2,1)} %gain.1, bf16[2,1024,512]{2,1,0:T(8,128)(2,1)} %rw.1, bf16[2,1024,512]{2,1,0:T(8,128)(2,1)} %kw.1, bf16[2,1024,512]{2,1,0:T(8,128)(2,1)} %vw.1, ...), custom_call_target="tpu_custom_call" | custom-call | tf_op jit(solution)/shard_map/two_blocks/pallas_call | solution.py:312
  29.9 1.4 %flush.1 = (bf16[16,1024]{1,0:T(8,128)(2,1)}, f32[2,4,8,64,64]{4,3,2,1,0:T(8,128)}) custom-call(bf16[16,1024]{1,0:T(8,128)(2,1)S(1)} %get-tuple-element.4.stream, f32[2,4,8,64,64]{4,3,2,1,0:T(8,128)S(1)} %get-tuple-element.5.states), custom_call_target="tpu_custom_call" | custom-call | tf_op jit(solution)/shard_map/flush/pallas_call | solution.py:355

commit v4 on v3

--- a/solution.py
+++ b/solution.py
@@ -46,11 +46,11 @@
     ]
     weights = (kw, rw, dw, tw, vw, gw)
     w_copy = [
-        [pltpu.make_async_copy(weights[r].at[l], w_v.at[l, r], w_sem.at[l, r]) for r in range(ROLES)]
+        [pltpu.make_async_copy(weights[r].at[l], w_v.at[l, r], w_sem.at[r]) for r in range(ROLES)]
         for l in range(layers)
     ]
-    ow_copy = [pltpu.make_async_copy(ow.at[l], ow_v.at[l], ow_sem.at[l]) for l in range(layers)]
-    s_copy = [pltpu.make_async_copy(states.at[l], s_v.at[l], s_sem.at[l]) for l in range(layers)]
+    ow_copy = [pltpu.make_async_copy(ow.at[l], ow_v.at[l], ow_sem) for l in range(layers)]
+    s_copy = [pltpu.make_async_copy(states.at[l], s_v.at[l], s_sem) for l in range(layers)]
     for copy in small:
         copy.start()
     for copy in w_copy[0]:
@@ -79,7 +79,7 @@
             [jnp.broadcast_to(row[:, g * LANES:(g + 1) * LANES], (local, LANES)) for g in range(groups)], axis=0
         )
 
-    started = []
+    sent = []
     for copy in small[:2]:
         copy.wait()
     chunks = br_s.shape[1]
@@ -96,33 +96,35 @@
         def send(src, dst, ss, rs, axis, index, size):
             for k in range(1, size):
                 peer = lax.rem(index + k, size)
+                slot = k - 1
                 if axis == "tp":
                     down, up = size - k, k - 1
                     down = jnp.where(down > index, down, down - 1)
                     up = jnp.where(up < index, up, up + 1)
                     peer = jnp.where(2 * index < size, down, up)
+                    slot = lax.rem(peer - index + size, size) - 1
                 copy = pltpu.make_async_remote_copy(
-                    src_ref=src(peer), dst_ref=dst(index), send_sem=ss.at[k], recv_sem=rs.at[index],
+                    src_ref=src(peer), dst_ref=dst(index), send_sem=ss.at[k - 1], recv_sem=rs.at[slot],
                     device_id={axis: peer}, device_id_type=MESH,
                 )
                 copy.start()
-                started.append(copy)
+                sent.append(copy)
 
         def receive(src, dst, ss, rs, axis, index, size):
             for k in range(1, size):
-                peer = lax.rem(index + k, size)
+                peer = lax.rem(index - k + size, size)
                 pltpu.make_async_remote_copy(
-                    src_ref=src(peer), dst_ref=dst(peer), send_sem=ss.at[k], recv_sem=rs.at[peer],
+                    src_ref=src(peer), dst_ref=dst(peer), send_sem=ss.at[k - 1], recv_sem=rs.at[k - 1],
                     device_id={axis: peer}, device_id_type=MESH,
                 ).wait_recv()
 
         sq_args = (
-            lambda p: sq_s.at[l, p], lambda p: sq_r.at[l, p], sq_ss.at[l], sq_rs.at[l], "dp", dp, n_dp,
+            lambda p: sq_s.at[l, p], lambda p: sq_r.at[l, p], sq_ss, sq_rs, "dp", dp, n_dp,
         )
         pj_args = [
             (
                 lambda p, c=c: proj_s.at[l, c, p], lambda p, c=c: proj_r.at[l, c, p],
-                pj_ss.at[l, c], pj_rs.at[l, c], "dp", dp, n_dp,
+                pj_ss.at[c], pj_rs.at[c], "dp", dp, n_dp,
             )
             for c in range(PAIRS)
         ]
@@ -147,6 +149,9 @@
                             parts.append(value)
                         else:
                             parts[r] = parts[r] + value
+        for copy in sent:
+            copy.wait_send()
+        sent.clear()
         wide = jnp.broadcast_to(square, (seqs, LANES))
         for d in range(n_dp):
             sq_s[l, d] = wide[d * local:(d + 1) * local]
@@ -181,7 +186,6 @@
                 for copy in w_copy[later]:
                     copy.start()
                 s_copy[later].start()
-                ow_copy[later].start()
 
         receive(*sq_args)
         total = sq_s[l, dp]
@@ -226,7 +230,7 @@
         normal = center * lax.rsqrt(head_sum(center * center) / head + 1e-05)
         mixed = normal * fold(hgain_v[l:l + 1, :].astype(F32)) * jax.nn.sigmoid(gate_pre)
         mix_s[l] = mixed.astype(BF16)
-        mx_args = (lambda p: mix_s.at[l], lambda p: mix_r.at[l, p], mx_ss.at[l], mx_rs.at[l], "dp", dp, n_dp)
+        mx_args = (lambda p: mix_s.at[l], lambda p: mix_r.at[l, p], mx_ss, mx_rs, "dp", dp, n_dp)
         send(*mx_args)
         mix_r[l, dp] = mix_s[l]
 
@@ -248,6 +252,8 @@
         renew(0, rows // 2)
 
         ow_copy[l].wait()
+        if l < layers - 1:
+            ow_copy[l + 1].start()
         receive(*mx_args)
         blocks = [mix_r[l, s].astype(F32) for s in range(n_dp)]
         gathered = jnp.concatenate(
@@ -260,7 +266,7 @@
         br_args = [
             (
                 lambda p, c=c: br_s.at[l, c], lambda p, c=c: br_r.at[l, p, c],
-                br_ss.at[l, c], br_rs.at[l, c], "tp", tp, n_tp,
+                br_ss.at[c], br_rs.at[l, c], "tp", tp, n_tp,
             )
             for c in range(chunks)
         ]
@@ -280,18 +286,14 @@
 
     for c in range(chunks):
         out_stream[:, spans[c]] = arrive(c).astype(BF16)
-    for copy in started:
+    for copy in sent:
         copy.wait_send()
 
 
 def flush(stream, states, out_stream, out_states, sem):
     copies = [pltpu.make_async_copy(stream, out_stream, sem.at[0])]
-    layers, local = states.shape[:2]
-    for l in range(layers):
-        for q in range(local):
-            copies.append(
-                pltpu.make_async_copy(states.at[l, q], out_states.at[l, q], sem.at[1 + l * local + q])
-            )
+    for l in range(states.shape[0]):
+        copies.append(pltpu.make_async_copy(states.at[l], out_states.at[l], sem.at[1 + l]))
     for copy in copies:
         copy.start()
     for copy in copies:
@@ -335,17 +337,17 @@
                 pltpu.VMEM((layers, chunks, seqs, cols // chunks), BF16),
                 pltpu.VMEM((layers, n_tp, chunks, seqs, cols // chunks), BF16),
                 dma((4,)),
-                dma((layers, ROLES)),
-                dma((layers,)),
-                dma((layers,)),
-                dma((layers, PAIRS, n_dp)),
-                dma((layers, PAIRS, n_dp)),
-                dma((layers, n_dp)),
-                dma((layers, n_dp)),
-                dma((layers, n_dp)),
-                dma((layers, n_dp)),
-                dma((layers, chunks, n_tp)),
-                dma((layers, chunks, n_tp)),
+                dma((ROLES,)),
+                dma,
+                dma,
+                dma((PAIRS, n_dp - 1)),
+                dma((PAIRS, n_dp - 1)),
+                dma((n_dp - 1,)),
+                dma((n_dp - 1,)),
+                dma((n_dp - 1,)),
+                dma((n_dp - 1,)),
+                dma((chunks, n_tp - 1)),
+                dma((layers, chunks, n_tp - 1)),
             ],
             compiler_params=pltpu.CompilerParams(
                 collective_id=0, has_side_effects=True, vmem_limit_bytes=56 * 1024 * 1024
@@ -360,7 +362,7 @@
             ),
             in_specs=[pl.BlockSpec(memory_space=pltpu.VMEM)] * 2,
             out_specs=(hbm_spec,) * 2,
-            scratch_shapes=[dma((1 + layers * local,))],
+            scratch_shapes=[dma((1 + layers,))],
             compiler_params=pltpu.CompilerParams(vmem_limit_bytes=1024 * 1024),
             name="flush",
         )(new_stream, new_states)

time: 31.5 us -> 30.8 us (0.978)
  Pallas kernels: 30.7 us -> 30 us
    pallas_call x1, Pallas kernels: 29.3 us -> 28.6 us  [per_device(): pl.pallas_call(functools.partial(kernel, n_dp, n_tp, cols * n_dp), out_sh...]
where the time goes in v4:
time: 30.8 us; the launch traced here: 30.6 us
  Pallas kernels  30 us (97%)
  between operations  0.64 us (2%)
    pallas_call x1, Pallas kernels, per_device(): pl.pallas_call(functools.partial(kernel, n_dp, n_tp, cols * n_dp), out_sh...  28.6 us
    pallas_call x1, Pallas kernels, per_device(): pl.pallas_call(flush, out_shape=(jax.ShapeDtypeStruct(stream.shape, BF16)...  1.35 us

profile of v4, /device:TPU:0, one launch (start us, length us, event | category | flops | bytes accessed | tf_op | source)
XLA Modules:
  0.0 30.6 jit_solution(591769628850654529)
XLA Ops:
  0.6 28.6 %two_blocks.1 = (bf16[16,1024]{1,0:T(8,128)(2,1)S(1)}, f32[2,4,8,64,64]{4,3,2,1,0:T(8,128)S(1)}) custom-call(bf16[16,1024]{1,0:T(8,128)(2,1)} %stream.1, f32[2,4,8,64,64]{4,3,2,1,0:T(8,128)} %states.1, bf16[2,1024]{1,0:T(2,128)(2,1)} %gain.1, bf16[2,1024,512]{2,1,0:T(8,128)(2,1)} %rw.1, bf16[2,1024,512]{2,1,0:T(8,128)(2,1)} %kw.1, bf16[2,1024,512]{2,1,0:T(8,128)(2,1)} %vw.1, ...), custom_call_target="tpu_custom_call" | custom-call | tf_op jit(solution)/shard_map/two_blocks/pallas_call | solution.py:314
  29.3 1.4 %flush.1 = (bf16[16,1024]{1,0:T(8,128)(2,1)}, f32[2,4,8,64,64]{4,3,2,1,0:T(8,128)}) custom-call(bf16[16,1024]{1,0:T(8,128)(2,1)S(1)} %get-tuple-element.4.stream, f32[2,4,8,64,64]{4,3,2,1,0:T(8,128)S(1)} %get-tuple-element.5.states), custom_call_target="tpu_custom_call" | custom-call | tf_op jit(solution)/shard_map/flush/pallas_call | solution.py:357
